TPU v7x, 32 devices: a whole 2x2x4 slice. The times are simulated.
32 devices in a mesh: sp: 4 (over y, x), tp: 8 (over z, core).
Axes of the slice: x: 2, y: 2, z: 4, core: 2. Of those that a mesh axis runs over, the one named last changes fastest.
Arguments:
- queries: bfloat16 [2048, 2048], P('sp', 'tp'), may hold values from -16 to 16
- key_vectors: bfloat16 [2048, 2048], P('sp', 'tp'), may hold values from -4 to 4
- value_vectors: bfloat16 [2048, 2048], P('sp', 'tp'), may hold values from -5 to 5
- forget_totals: float32 [2048, 16], P('sp', 'tp'), may hold values from -344 to 0, as said below
- head_gain: float32 [2048], P('tp'), may hold values from 0.1 to 1.9
- stream: bfloat16 [2048, 2048], P(('sp', 'tp')), may hold values from -6 to 6
- out_weight: bfloat16 [2048, 2048], replicated, may hold values from -0.125 to 0.125
- norm_gain: float32 [2048], replicated, may hold values from 0.1 to 1.9
- routing: int32 [2048, 2], P(('sp', 'tp')), may hold values from 0 to 3, all different within a row; in each aligned block of 64 rows (0 to 63, 64 to 127, ...) at most 64 rows name the same one
- route_weights: float32 [2048, 2], P(('sp', 'tp')), may hold values from 0.2 to 1
- gate_weight: bfloat16 [4, 2048, 4096], P('sp', None, 'tp'), may hold values from -0.125 to 0.125
- up_weight: bfloat16 [4, 2048, 4096], P('sp', None, 'tp'), may hold values from -0.125 to 0.125
- down_weight: bfloat16 [4, 4096, 2048], P('sp', 'tp'), may hold values from -0.09375 to 0.09375
Outputs:
- layer_out: bfloat16 [2048, 2048], P(('sp', 'tp'))
Inputs may be any that keep to these rules, and one draw needn't show every extreme that they name: `forget_totals`: along the positions, the values of each head never rise. `routing`: A token's 2 experts differ. Within the tokens of one device (aligned blocks of 64 rows) no expert is named more than 64 times.
All inputs are finite; a program needn't handle non-finite values.
Results may differ from a plain program's by a relative error of at most 0.01145.
Values may be sent and summed in bfloat16 or wider, within the bound.
A program may use at most 128 MiB of HBM per device.

v0:
```python
from functools import partial

import jax
import jax.numpy as jnp
from jax import lax
from jax.sharding import PartitionSpec as P

HD = 128
TOP = 2


masked_score = -1e30


def attend_block(
    totals, query_rows, query_gate, query_pos, key_rows, value_rows, key_gate, key_pos
):
    run_max, run_sum, run_acc = totals
    scores = jnp.einsum("qhd,khd->hqk", query_rows, key_rows, preferred_element_type=jnp.float32)
    scores = scores * HD ** (-0.5) + query_gate[:, :, None] - key_gate[:, None, :]
    visible = (key_pos[None, :] <= query_pos[:, None])[None]
    scores = jnp.where(visible, scores, masked_score)
    new_max = jnp.maximum(run_max, jnp.max(scores, axis=2))
    lifted = jnp.where(visible, jnp.exp(scores - new_max[:, :, None]), 0.0)
    rescale = jnp.exp(run_max - new_max)
    new_sum = run_sum * rescale + jnp.sum(lifted, axis=2)
    product = jnp.einsum(
        "hqk,khd->hqd", lifted.astype(jnp.bfloat16), value_rows, preferred_element_type=jnp.float32
    )
    new_acc = run_acc * rescale[:, :, None] + product
    return (new_max, new_sum, new_acc)


def keep_totals(totals_in):
    return totals_in


def make_folder(segments, gathered_gates):

    def fold_keys(state_all, key_piece, first_key):
        key_part, value_part = key_piece
        key_total = key_part.shape[0]
        block_len = min(512, key_total)
        heads_dev = segments[0][0].shape[1]
        key_part = key_part.reshape(key_total, heads_dev, HD)
        value_part = value_part.reshape(key_total, heads_dev, HD)

        def one_block(block_index, state_now):
            offset = block_index * block_len
            key_rows = lax.dynamic_slice_in_dim(key_part, offset, block_len, 0)
            value_rows = lax.dynamic_slice_in_dim(value_part, offset, block_len, 0)
            key_pos = offset + jnp.arange(block_len, dtype=jnp.int32)
            key_gate = jnp.transpose(lax.dynamic_slice_in_dim(gathered_gates, offset, block_len, 0))
            updated = []
            for segment, totals_in in zip(segments, state_now):
                query_rows, query_gate, query_pos = segment
                needed = offset <= query_pos[-1]
                advance = partial(
                    attend_block,
                    query_rows=query_rows,
                    query_gate=query_gate,
                    query_pos=query_pos,
                    key_rows=key_rows,
                    value_rows=value_rows,
                    key_gate=key_gate,
                    key_pos=key_pos,
                )
                updated.append(lax.cond(needed, advance, keep_totals, totals_in))
            return tuple(updated)

        return lax.fori_loop(0, key_total // block_len, one_block, state_all)

    return fold_keys


def on_device(
    queries,
    key_vectors,
    value_vectors,
    forget_totals,
    head_gain,
    stream,
    out_weight,
    norm_gain,
    routing,
    route_weights,
    gate_weight,
    up_weight,
    down_weight,
):
    tok_count = queries.shape[0]
    heads_dev = queries.shape[1] // HD
    sp_index = lax.axis_index("sp")
    sp_count = lax.axis_size("sp")
    gathered_gates = lax.all_gather(forget_totals, "sp", axis=0, tiled=True)
    first_pos = sp_index * tok_count
    query_pos = first_pos + jnp.arange(tok_count, dtype=jnp.int32)
    query_gate = jnp.transpose(lax.dynamic_slice_in_dim(gathered_gates, first_pos, tok_count, 0))
    segments = [(queries.reshape(tok_count, heads_dev, HD), query_gate, query_pos)]
    starting = (
        (
            jnp.full((heads_dev, tok_count), masked_score, jnp.float32),
            jnp.zeros((heads_dev, tok_count), jnp.float32),
            jnp.zeros((heads_dev, tok_count, HD), jnp.float32),
        ),
    )
    folder = make_folder(segments, gathered_gates)
    totals = folder(
        starting,
        (
            lax.all_gather(key_vectors, "sp", axis=0, tiled=True),
            lax.all_gather(value_vectors, "sp", axis=0, tiled=True),
        ),
        jnp.int32(0),
    )
    run_max, run_sum, run_acc = totals[0]
    attended = run_acc / run_sum[:, :, None]
    inverse_rms = lax.rsqrt(jnp.mean(attended * attended, axis=2, keepdims=True) + 1e-06)
    normed = attended * inverse_rms * head_gain.reshape(heads_dev, 1, HD)
    head_out = (
        jnp.transpose(normed, (1, 0, 2)).reshape(tok_count, heads_dev * HD).astype(jnp.bfloat16)
    )
    token_heads = lax.all_to_all(head_out, "tp", split_axis=0, concat_axis=1, tiled=True)
    mixed_rows = jnp.dot(token_heads, out_weight, preferred_element_type=jnp.float32)
    resid_sum = stream.astype(jnp.float32) + mixed_rows
    center = resid_sum - jnp.mean(resid_sum, axis=1, keepdims=True)
    normed_rows = (
        center * lax.rsqrt(jnp.mean(center * center, axis=1, keepdims=True) + 1e-05) * norm_gain
    ).astype(jnp.bfloat16)
    row_count = normed_rows.shape[0]
    capacity = max(2, 2 * TOP * row_count // sp_count)
    flat_expert = routing.reshape(-1)
    onehot = (flat_expert[:, None] == jnp.arange(sp_count, dtype=jnp.int32)[None, :]).astype(
        jnp.int32
    )
    earlier = jnp.cumsum(onehot, axis=0) - onehot
    slot_index = flat_expert * capacity + jnp.sum(earlier * onehot, axis=1)
    slot_grid = slot_index.reshape(row_count, TOP)
    slot_ids = jnp.arange(sp_count * capacity, dtype=jnp.int32)
    placing = jnp.sum(
        (slot_grid[None, :, :] == slot_ids[:, None, None]).astype(jnp.float32), axis=2
    ).astype(jnp.bfloat16)
    outgoing = jnp.dot(placing, normed_rows, preferred_element_type=jnp.float32).astype(
        jnp.bfloat16
    )
    outgoing = outgoing.reshape(sp_count, capacity, normed_rows.shape[1])
    arrived = lax.all_to_all(outgoing, "sp", split_axis=0, concat_axis=0, tiled=True)
    row_piece = lax.all_gather(arrived.reshape(-1, arrived.shape[2]), "tp", axis=0, tiled=True)
    gate_pre = jnp.dot(row_piece, gate_weight[0], preferred_element_type=jnp.float32)
    up_pre = jnp.dot(row_piece, up_weight[0], preferred_element_type=jnp.float32)
    hidden = (jax.nn.silu(gate_pre) * up_pre).astype(jnp.bfloat16)
    summed = lax.psum_scatter(
        jnp.dot(hidden, down_weight[0], preferred_element_type=jnp.float32).astype(jnp.bfloat16),
        "tp",
        scatter_dimension=0,
        tiled=True,
    )
    expert_out = summed.reshape(sp_count, capacity, -1)
    returned = lax.all_to_all(expert_out, "sp", split_axis=0, concat_axis=0, tiled=True)
    picked = returned.reshape(sp_count * capacity, -1)[slot_index].astype(jnp.float32)
    weighted = picked * route_weights.reshape(-1)[:, None]
    routed = jnp.sum(weighted.reshape(row_count, TOP, -1), axis=1)
    return (resid_sum + routed).astype(jnp.bfloat16)


def solution(mesh):
    in_specs = (
        P("sp", "tp"),
        P("sp", "tp"),
        P("sp", "tp"),
        P("sp", "tp"),
        P("tp"),
        P(("sp", "tp"), None),
        P(),
        P(),
        P(("sp", "tp"), None),
        P(("sp", "tp"), None),
        P("sp", None, "tp"),
        P("sp", None, "tp"),
        P("sp", "tp", None),
    )
    out_specs = P(("sp", "tp"), None)
    return jax.shard_map(
        on_device, mesh=mesh, in_specs=in_specs, out_specs=out_specs, check_vma=False
    )
```

profile of v0, /device:TPU:0, one launch (start us, length us, event | category | flops | bytes accessed | tf_op | source)
XLA Modules:
  0.0 348.3 jit_solution(13763820475553756296)
XLA Ops:
  6.5 1.9 copy.31
  8.6 1.8 copy.33
  11.9 9.7 %all_gather.12 = f32[2048,2]{0,1:T(2,128)S(1)} all-gather(f32[512,2]{0,1:T(2,128)S(1)} %copy-done.5), channel_id=1, replica_groups=mesh['sp'=4,'tp'=8] {'sp'}, dimensions={0}, use_global_device_ids=true | all-gather | bytes 20480 | tf_op jit(solution)/shard_map/all_gather | solution.py:95
  21.6 16.7 %all-gather.4.cloned.1.call-done = bf16[2048,256]{0,1:T(8,128)(2,1)} async-done(((bf16[512,256]{0,1:T(8,128)(2,1)}), bf16[2048,256]{0,1:T(8,128)(2,1)}) %all-gather.4.cloned.1.call-update) | async-done | bytes 1048592 | tf_op jit(solution)/shard_map/all_gather | solution.py:111
  38.3 2.3 copy.34
  40.5 26.0 %all-gather.6.cloned.1.call-done = bf16[2048,256]{0,1:T(8,128)(2,1)} async-done(((bf16[512,256]{0,1:T(8,128)(2,1)}), bf16[2048,256]{0,1:T(8,128)(2,1)}) %all-gather.6.cloned.1.call-update) | async-done | bytes 1048592 | tf_op jit(solution)/shard_map/all_gather | solution.py:112
  66.5 2.3 copy.36
  68.9 9.9 %while.17 = (s32[]{:T(128)}, f32[2,512]{1,0:T(2,128)S(1)}, f32[2,512]{1,0:T(2,128)S(1)}, f32[2,512,128]{2,1,0:T(8,128)S(1)}, s32[512]{0:T(512)S(1)}, /*index=5*/...) while((s32[]{:T(128)}, f32[2,512]{1,0:T(2,128)S(1)}, ...), condition=%wide.region_5.6_spmd, body=%wide.region_0.5_spmd.sunk | while | flops 274729472 | bytes 9268585 | solution.py:71
  70.2 4.3 %conditional.2 = ((f32[2,512]{1,0:T(2,128)S(1)}, f32[2,512]{1,0:T(2,128)S(1)}, f32[2,512,128]{2,1,0:T(8,128)S(1)})) conditional(s32[]{:T(128)} %convert_element_type.90, (f32[2,512]{1,0:T(2,128)S(1)}, f32[2,512]{1,0:T(2,128)S(1)}, f32[2,512,128]{2,1,0:T(8,128)S(1)}) %tuple.47, (s32[]{:T(128)}, s32[512]{0:T(512)S(1)}, s32[512]{0:T(512)S(1)}, ...), branch_computations={%region_1.0_spmd, %region_2.4_spmd} | conditional | flops 274729472 | bytes 9258020 | solution.py:68
  72.6 1.9 convolution_add_fusion
  80.7 4.6 %all-to-all-start = ((bf16[8,64,256]{2,1,0:T(8,128)(2,1)}), bf16[8,64,256]{2,1,0:T(8,128)(2,1)S(1)}, u32[]{:S(2)}, u32[]{:S(2)}) async-start(bf16[8,64,256]{2,1,0:T(8,128)(2,1)} %convert_element_type.59), calls=%async_computation | async-start | bytes 524288 | tf_op jit(solution)/shard_map/all_to_all | solution.py:123
  86.1 8.9 %all-to-all-done = bf16[8,64,256]{2,1,0:T(8,128)(2,1)S(1)} async-done(((bf16[8,64,256]{2,1,0:T(8,128)(2,1)}), bf16[8,64,256]{2,1,0:T(8,128)(2,1)S(1)}, u32[]{:S(2)}, u32[]{:S(2)}) %all-to-all-start) | async-done | bytes 262176 | tf_op jit(solution)/shard_map/all_to_all | solution.py:123
  95.0 5.1 %fusion.24 = (f32[64]{0:T(128)S(1)}, f32[64,2048]{1,0:T(8,128)S(1)}) fusion(bf16[64,2048]{1,0:T(8,128)(2,1)S(1)} %bitcast.49, bf16[2048,2048]{1,0:T(8,128)(2,1)} %param.23, bf16[64,2048]{1,0:T(8,128)(2,1)S(1)} %copy-done.3), kind=kOutput, calls=%fused_computation.56 | convolution fusion | flops 537264064 | bytes 9437440 | tf_op jit(solution)/shard_map/dot_general | solution.py:124
  100.9 29.2 %all_to_all.26 = bf16[4,64,2048]{2,1,0:T(8,128)(2,1)} all-to-all(bf16[4,64,2048]{2,1,0:T(8,128)(2,1)S(1)} %bitcast.48), channel_id=1, replica_groups=mesh['sp'=4,'tp'=8] {'sp'}, dimensions={0} | all-to-all | bytes 2097152 | tf_op jit(solution)/shard_map/all_to_all | solution.py:147
  130.3 80.0 %all-gather.8.cloned.1.call-done = bf16[2048,2048]{1,0:T(8,128)(2,1)} async-done(((bf16[256,2048]{1,0:T(8,128)(2,1)}), bf16[2048,2048]{1,0:T(8,128)(2,1)}) %all-gather.8.cloned.1.call-update) | async-done | bytes 8388624 | tf_op jit(solution)/shard_map/all_gather | solution.py:148
  210.3 7.7 %fusion.13 = f32[2048,512]{1,0:T(8,128)S(1)} fusion(bf16[2048,2048]{1,0:T(8,128)(2,1)} %all-gather.8.cloned.1.call-done, bf16[1,2048,512]{2,1,0:T(8,128)(2,1)} %param.27), kind=kOutput, calls=%fused_computation.25 | convolution fusion | flops 4294967296 | bytes 14680064 | tf_op jit(solution)/shard_map/dot_general | solution.py:149
  218.0 5.2 %multiply_convert_fusion = bf16[2048,512]{1,0:T(8,128)(2,1)S(1)} fusion(f32[2048,512]{1,0:T(8,128)S(1)} %fusion.13, bf16[2048,2048]{1,0:T(8,128)(2,1)S(1)} %copy-done.9, bf16[1,2048,512]{2,1,0:T(8,128)(2,1)S(1)} %copy-done.10), kind=kOutput, calls=%fused_computation.20 | convolution fusion | flops 4301258752 | bytes 16777216 | tf_op jit(solution)/shard_map/dot_general | solution.py:150
  223.2 6.8 %convolution_convert_fusion = bf16[2048,2048]{1,0:T(8,128)(2,1)} fusion(bf16[2048,512]{1,0:T(8,128)(2,1)S(1)} %multiply_convert_fusion, bf16[1,512,2048]{2,1,0:T(8,128)(2,1)S(1)} %copy-done), kind=kOutput, calls=%fused_computation.19 | convolution fusion | flops 4299161600 | bytes 12582912 | tf_op jit(solution)/shard_map/dot_general | solution.py:153
  230.0 88.2 %reduce-scatter.2.cloned.1.call-done = bf16[256,2048]{1,0:T(8,128)(2,1)} async-done(((bf16[2048,2048]{1,0:T(8,128)(2,1)}), bf16[256,2048]{1,0:T(8,128)(2,1)}) %reduce-scatter.2.cloned.1.call-update) | async-done | bytes 1048592 | tf_op jit(solution)/shard_map/reduce_scatter | solution.py:152
  318.2 3.6 %all-to-all-start.2 = ((bf16[4,64,2048]{2,1,0:T(8,128)(2,1)}), bf16[4,64,2048]{2,1,0:T(8,128)(2,1)S(1)}, u32[]{:S(2)}, u32[]{:S(2)}) async-start(bf16[4,64,2048]{2,1,0:T(8,128)(2,1)} %bitcast.52), calls=%async_computation.3 | async-start | bytes 2097152 | tf_op jit(solution)/shard_map/all_to_all | solution.py:159
  322.1 11.6 %all-to-all-done.2 = bf16[4,64,2048]{2,1,0:T(8,128)(2,1)S(1)} async-done(((bf16[4,64,2048]{2,1,0:T(8,128)(2,1)}), bf16[4,64,2048]{2,1,0:T(8,128)(2,1)S(1)}, u32[]{:S(2)}, u32[]{:S(2)}) %all-to-all-start.2) | async-done | bytes 1048608 | tf_op jit(solution)/shard_map/all_to_all | solution.py:159
  333.7 1.7 gather_fusion
  335.5 2.7 reshape.135
  338.2 2.8 multiply_reduce_fusion
  (83 shorter events, 11.4 us)
Async XLA Ops:
  6.5 216.6 %copy-start = (bf16[1,512,2048]{2,1,0:T(8,128)(2,1)S(1)}, bf16[1,512,2048]{2,1,0:T(8,128)(2,1)}, u32[]{:S(2)}) copy-start(bf16[1,512,2048]{2,1,0:T(8,128)(2,1)} %param.29) | copy-start | bytes 6291460
  6.5 5.1 %copy-start.7 = (s32[64,2]{0,1:T(2,128)S(1)}, s32[64,2]{0,1:T(2,128)}, u32[]{:S(2)}) copy-start(s32[64,2]{0,1:T(2,128)} %param.25) | copy-start | bytes 1540
  6.5 5.4 %copy-start.5 = (f32[512,2]{0,1:T(2,128)S(1)}, f32[512,2]{0,1:T(2,128)}, u32[]{:S(2)}) copy-start(f32[512,2]{0,1:T(2,128)} %param.20) | copy-start | bytes 12292
  6.5 31.7 %all-gather.4.cloned.1.call-start = ((), (), s32[]{:S(2)}) async-start(), calls=%async_computation.4 | async-start | bytes 1310720 | tf_op jit(solution)/shard_map/all_gather | solution.py:111
  8.5 58.0 %all-gather.6.cloned.1.call-start = ((), (), s32[]{:S(2)}) async-start(), calls=%async_computation.5 | async-start | bytes 1310720 | tf_op jit(solution)/shard_map/all_gather | solution.py:112
  68.8 10.3 %copy-start.6 = (f32[256]{0:T(256)S(1)}, f32[256]{0:T(256)}, u32[]{:S(2)}) copy-start(f32[256]{0:T(256)} %param.21) | copy-start | bytes 3076
  78.7 16.3 %copy-start.3 = (bf16[64,2048]{1,0:T(8,128)(2,1)S(1)}, bf16[64,2048]{1,0:T(8,128)(2,1)}, u32[]{:S(2)}) copy-start(bf16[64,2048]{1,0:T(8,128)(2,1)} %param.22) | copy-start | bytes 786436
  80.7 14.3 %all-to-all-start = ((bf16[8,64,256]{2,1,0:T(8,128)(2,1)}), bf16[8,64,256]{2,1,0:T(8,128)(2,1)S(1)}, u32[]{:S(2)}, u32[]{:S(2)}) async-start(bf16[8,64,256]{2,1,0:T(8,128)(2,1)} %convert_element_type.59), calls=%async_computation | async-start | bytes 524288 | tf_op jit(solution)/shard_map/all_to_all | solution.py:123
  85.3 125.0 %all-gather.8.cloned.1.call-start = ((), (), s32[]{:S(2)}) async-start(), calls=%async_computation.6 | async-start | bytes 9437184 | tf_op jit(solution)/shard_map/all_gather | solution.py:148
  95.0 5.3 %copy-start.4 = (f32[2048]{0:T(1024)S(1)}, f32[2048]{0:T(1024)}, u32[]{:S(2)}) copy-start(f32[2048]{0:T(1024)} %param.24) | copy-start | bytes 24580
  100.1 29.9 %copy-start.1 = (f32[64,2048]{1,0:T(8,128)}, f32[64,2048]{1,0:T(8,128)S(1)}, u32[]{:S(2)}) copy-start(f32[64,2048]{1,0:T(8,128)S(1)} %get-tuple-element.334) | copy-start | bytes 1572868
  130.1 188.1 %reduce-scatter.2.cloned.1.call-start = ((), (), s32[]{:S(2)}) async-start(), calls=%async_computation.7 | async-start | bytes 9437184 | tf_op jit(solution)/shard_map/reduce_scatter | solution.py:152
  210.3 7.7 %copy-start.9 = (bf16[2048,2048]{1,0:T(8,128)(2,1)S(1)}, bf16[2048,2048]{1,0:T(8,128)(2,1)}, u32[]{:S(2)}) copy-start(bf16[2048,2048]{1,0:T(8,128)(2,1)} %all-gather.8.cloned.1.call-done) | copy-start | bytes 25165828
  210.3 7.7 %copy-start.10 = (bf16[1,2048,512]{2,1,0:T(8,128)(2,1)S(1)}, bf16[1,2048,512]{2,1,0:T(8,128)(2,1)}, u32[]{:S(2)}) copy-start(bf16[1,2048,512]{2,1,0:T(8,128)(2,1)} %param.28) | copy-start | bytes 6291460
  230.0 92.0 %copy-start.8 = (f32[64,2]{0,1:T(2,128)S(1)}, f32[64,2]{0,1:T(2,128)}, u32[]{:S(2)}) copy-start(f32[64,2]{0,1:T(2,128)} %param.26) | copy-start | bytes 1540
  318.2 15.5 %all-to-all-start.2 = ((bf16[4,64,2048]{2,1,0:T(8,128)(2,1)}), bf16[4,64,2048]{2,1,0:T(8,128)(2,1)S(1)}, u32[]{:S(2)}, u32[]{:S(2)}) async-start(bf16[4,64,2048]{2,1,0:T(8,128)(2,1)} %bitcast.52), calls=%async_computation.3 | async-start | bytes 2097152 | tf_op jit(solution)/shard_map/all_to_all | solution.py:159
  335.5 5.5 %copy-start.2 = (f32[64,2048]{1,0:T(8,128)S(1)}, f32[64,2048]{1,0:T(8,128)}, u32[]{:S(2)}) copy-start(f32[64,2048]{1,0:T(8,128)} %copy-done.1) | copy-start | bytes 1572868
Sparse Core Ops, SparseCore 0:
  9.2 29.0 all-gather.3
  40.1 26.3 all-gather.5
  130.2 80.0 all-gather.7
  230.1 88.0 reduce-scatter.1
where the time goes:
time: 349 us; the launch traced here: 348 us
  waiting for transfers between devices  231 us (66%)
  blocking collectives  38.8 us (11%)
  matrix products  28.8 us (8%)
  local copies, waits for them, and re-layouts  18.6 us (5%)
  between operations  13.4 us (4%)
  starting transfers between devices  8.56 us (2%)
  other arithmetic  5.73 us (2%)
    reduce_scatter x1, waiting for transfers between devices, on_device(): lax.psum_scatter(jnp.dot(hidden, down_weight[0], preferred_element_type=j...  88.2 us
    all_gather x1, waiting for transfers between devices, on_device(): lax.all_gather(arrived.reshape(-1, arrived.shape[2]), 'tp', axis=0, tiled...  80 us
    all_to_all x1, blocking collectives, on_device(): lax.all_to_all(outgoing, 'sp', split_axis=0, concat_axis=0, tiled=True)  29.2 us
    all_gather x1, waiting for transfers between devices, on_device(): lax.all_gather(value_vectors, 'sp', axis=0, tiled=True)  26 us
    all_gather x1, waiting for transfers between devices, on_device(): lax.all_gather(key_vectors, 'sp', axis=0, tiled=True)  16.7 us
    all_to_all x1, waiting for transfers between devices, on_device(): lax.all_to_all(expert_out, 'sp', split_axis=0, concat_axis=0, tiled=True)  11.6 us
    all_gather x1, blocking collectives, on_device(): gathered_gates = lax.all_gather(forget_totals, 'sp', axis=0, tiled=True)  9.67 us
    all_to_all x1, waiting for transfers between devices, on_device(): lax.all_to_all(head_out, 'tp', split_axis=0, concat_axis=1, tiled=True)  8.89 us
  transfers between devices with their start and end apart: 6, of which 6 were waited for; matrix products, arithmetic and copies ran while one was open for 2% of the time, Pallas kernels for 0%

commit v1 on v0

--- a/solution.py
+++ b/solution.py
@@ -3,6 +3,8 @@
 import jax
 import jax.numpy as jnp
 from jax import lax
+from jax.experimental import pallas as pl
+from jax.experimental.pallas import tpu as pltpu
 from jax.sharding import PartitionSpec as P
 
 HD = 128
@@ -71,6 +73,342 @@
         return lax.fori_loop(0, key_total // block_len, one_block, state_all)
 
     return fold_keys
+
+
+MESH = pl.DeviceIdType.MESH
+LANES = 128
+QUADS = 4
+
+
+def z_steps(depth):
+    steps = []
+    for near in range(1, depth // 2 + 1):
+        for step in (near, depth - near):
+            if step not in steps:
+                steps.append(step)
+    return steps
+
+
+def experts_kernel(
+    depth,
+    own_rows,
+    resid,
+    gate_hbm,
+    up_hbm,
+    down_hbm,
+    out_ref,
+    rows_all,
+    gate_w,
+    up_w,
+    down_w,
+    hidden,
+    mine,
+    theirs,
+    from_core,
+    from_second,
+    from_first,
+    from_z,
+    local_sems,
+    ag_send_sems,
+    ag_recv_sems,
+    rs_send_sems,
+    core_sems,
+    second_sems,
+    first_sems,
+    z_sems,
+):
+    sp = lax.axis_index("sp")
+    tp = lax.axis_index("tp")
+    width = resid.shape[1]
+    count = resid.shape[0]
+    z, core = tp // 2, tp % 2
+    other = 1 - core
+    x_next = sp + 1 - 2 * (sp % 2)
+    y_next = (sp + 2) % 4
+    first = x_next * (1 - core) + y_next * core
+    second = y_next * (1 - core) + x_next * core
+    far = 3 - sp
+    to_core = (sp, z * 2 + other)
+    to_first = (first, tp)
+    to_second = (second, tp)
+
+    def to_z(step):
+        return (sp, ((z + step) % depth) * 2 + core)
+
+    steps = z_steps(depth)
+    loads = [
+        pltpu.make_async_copy(own_rows, rows_all.at[core * QUADS + sp, z], local_sems.at[0]),
+        pltpu.make_async_copy(gate_hbm.at[0], gate_w, local_sems.at[1]),
+        pltpu.make_async_copy(up_hbm.at[0], up_w, local_sems.at[2]),
+        pltpu.make_async_copy(down_hbm.at[0], down_w, local_sems.at[3]),
+    ]
+    for load in loads:
+        load.start()
+
+    barrier = pltpu.get_barrier_semaphore()
+    peers = [to_core, to_first, to_second] + [to_z(step) for step in steps]
+    for peer in peers:
+        pl.semaphore_signal(barrier, inc=1, device_id=peer, device_id_type=MESH)
+    pl.semaphore_wait(barrier, len(peers))
+
+    started = []
+
+    def spread(src, group, zz, target):
+        copy = pltpu.make_async_remote_copy(
+            src_ref=src,
+            dst_ref=rows_all.at[group, zz],
+            send_sem=ag_send_sems.at[len(started)],
+            recv_sem=ag_recv_sems.at[group, zz],
+            device_id=target,
+            device_id_type=MESH,
+        )
+        copy.start()
+        started.append(copy)
+
+    def arrived(group, zz):
+        slot = rows_all.at[group, zz]
+        pltpu.make_async_remote_copy(
+            src_ref=slot,
+            dst_ref=slot,
+            send_sem=ag_send_sems.at[0],
+            recv_sem=ag_recv_sems.at[group, zz],
+            device_id=to_core,
+            device_id_type=MESH,
+        ).wait_recv()
+
+    def onward(group, zz, targets):
+        arrived(group, zz)
+        for target in targets:
+            spread(rows_all.at[group, zz], group, zz, target)
+
+    def from_partner(quad):
+        for zz in range(depth):
+            arrived(other * QUADS + quad, zz)
+
+    def experts(group, dest, quad):
+        half = 256 if gate_w.shape[1] % 256 == 0 else gate_w.shape[1]
+
+        @pl.loop(0, gate_w.shape[1] // half)
+        def _(j):
+            cols = pl.ds(pl.multiple_of(j * half, half), half)
+            block = rows_all[group, :, :, :width].reshape(depth * count, width)
+            gate_pre = jnp.dot(block, gate_w[:, cols], preferred_element_type=jnp.float32)
+            up_pre = jnp.dot(block, up_w[:, cols], preferred_element_type=jnp.float32)
+            hidden[:, cols] = (gate_pre / (1.0 + jnp.exp(-gate_pre)) * up_pre).astype(jnp.bfloat16)
+
+        pieces = rows_all[group, :, :, width:].reshape(depth * count, LANES).astype(jnp.float32)
+        lane = lax.broadcasted_iota(jnp.int32, pieces.shape, 1)
+        weight = jnp.sum(jnp.where(lane % QUADS == sp, pieces, 0.0), axis=1, keepdims=True)
+        step = 512 if width % 512 == 0 else width
+
+        @pl.loop(0, width // step)
+        def _(j):
+            cols = pl.ds(pl.multiple_of(j * step, step), step)
+            product = jnp.dot(hidden[...], down_w[:, cols], preferred_element_type=jnp.float32)
+            dest[quad, :, :, cols] = (
+                (product * weight).astype(jnp.bfloat16).reshape(depth, count, step)
+            )
+
+    returned = []
+
+    def send_back(src, dst, sem, target):
+        copy = pltpu.make_async_remote_copy(
+            src_ref=src,
+            dst_ref=dst,
+            send_sem=rs_send_sems.at[len(returned)],
+            recv_sem=sem,
+            device_id=target,
+            device_id_type=MESH,
+        )
+        copy.start()
+        returned.append(copy)
+
+    def landed(dst, sem):
+        pltpu.make_async_remote_copy(
+            src_ref=dst,
+            dst_ref=dst,
+            send_sem=rs_send_sems.at[0],
+            recv_sem=sem,
+            device_id=to_core,
+            device_id_type=MESH,
+        ).wait_recv()
+
+    def partner_part(quad):
+        experts(other * QUADS + quad, theirs, quad)
+        send_back(theirs.at[quad], from_core.at[quad], core_sems.at[quad], to_core)
+
+    def f32(value):
+        return value.astype(jnp.float32)
+
+    own_group = core * QUADS + sp
+    for target in [to_z(step) for step in steps] + [to_first, to_second, to_core]:
+        spread(own_rows, own_group, z, target)
+    before = None
+    for step in [0] + steps + [None]:
+        if step:
+            onward(own_group, (z - step + depth) % depth, [to_first, to_second, to_core])
+        if before is not None:
+            zz = (z - before + depth) % depth
+            onward(core * QUADS + first, zz, [to_second, to_core])
+        before = step
+    for load in loads:
+        load.wait()
+    order = [0] + steps
+    experts(own_group, mine, sp)
+    from_partner(sp)
+    partner_part(sp)
+    for step in order:
+        onward(core * QUADS + second, (z - step + depth) % depth, [to_core])
+    experts(core * QUADS + first, mine, first)
+    from_partner(second)
+    partner_part(second)
+    experts(core * QUADS + second, mine, second)
+    from_partner(first)
+    partner_part(first)
+
+    back_steps = steps + [0]
+
+    def hand_over(quad, slot):
+        landed(from_core.at[quad], core_sems.at[quad])
+        mine[quad] = (f32(mine[quad]) + f32(from_core[quad])).astype(jnp.bfloat16)
+        for step in back_steps:
+            zz = (z + step) % depth
+            send_back(
+                mine.at[quad, zz], from_second.at[slot, zz], second_sems.at[slot, zz], to_second
+            )
+
+    hand_over(second, 0)
+    for step in order:
+        onward(core * QUADS + far, (z - step + depth) % depth, [to_core])
+    experts(core * QUADS + far, mine, far)
+    from_partner(far)
+    partner_part(far)
+    hand_over(far, 1)
+
+    landed(from_core.at[first], core_sems.at[first])
+    landed(from_core.at[sp], core_sems.at[sp])
+    for step in back_steps:
+        zz = (z + step) % depth
+        landed(from_second.at[1, zz], second_sems.at[1, zz])
+        mine[first, zz] = (
+            f32(mine[first, zz]) + f32(from_core[first, zz]) + f32(from_second[1, zz])
+        ).astype(jnp.bfloat16)
+        send_back(mine.at[first, zz], from_first.at[zz], first_sems.at[zz], to_first)
+    for step in back_steps:
+        zz = (z + step) % depth
+        landed(from_second.at[0, zz], second_sems.at[0, zz])
+        landed(from_first.at[zz], first_sems.at[zz])
+        total = (
+            f32(mine[sp, zz])
+            + f32(from_core[sp, zz])
+            + f32(from_second[0, zz])
+            + f32(from_first[zz])
+        )
+        if step:
+            mine[sp, zz] = total.astype(jnp.bfloat16)
+            send_back(mine.at[sp, zz], from_z.at[step - 1], z_sems.at[step - 1], to_z(step))
+        else:
+            total = resid[...] + total
+            for slot in range(depth - 1):
+                landed(from_z.at[slot], z_sems.at[slot])
+                total = total + f32(from_z[slot])
+            out_ref[...] = total.astype(out_ref.dtype)
+    for copy in started + returned:
+        copy.wait_send()
+
+
+def dense_experts(
+    resid_sum, normed_rows, routing, route_weights, gate_weight, up_weight, down_weight
+):
+    depth = lax.axis_size("tp") // 2
+    count, width = normed_rows.shape
+    units = gate_weight.shape[2]
+    experts = jnp.arange(QUADS, dtype=jnp.int32)
+    named = routing[:, :, None] == experts[None, None, :]
+    weights = jnp.sum(jnp.where(named, route_weights[:, :, None], 0.0), axis=1)
+    high = lax.reduce_precision(weights, 8, 7)
+    middle = lax.reduce_precision(weights - high, 8, 7)
+    low = weights - high - middle
+    pieces = jnp.concatenate([high, middle, low], axis=1).astype(jnp.bfloat16)
+    pieces = jnp.pad(pieces, ((0, 0), (0, LANES - pieces.shape[1])))
+    extended = jnp.concatenate([normed_rows, pieces], axis=1)
+    bf16 = jnp.bfloat16
+    dma = pltpu.SemaphoreType.DMA
+    block = (depth, count, width)
+    vmem = pl.BlockSpec(memory_space=pltpu.VMEM)
+    hbm = pl.BlockSpec(memory_space=pl.ANY)
+    ag_sends = (depth - 1 + 3) + 3 * (depth - 1) + 2 * depth + 2 * depth
+    rs_sends = QUADS + 2 * depth + depth + depth - 1
+    return pl.pallas_call(
+        partial(experts_kernel, depth),
+        out_shape=jax.ShapeDtypeStruct((count, width), bf16),
+        in_specs=[vmem, vmem, hbm, hbm, hbm],
+        out_specs=vmem,
+        scratch_shapes=[
+            pltpu.VMEM((2 * QUADS, depth, count, width + LANES), bf16),
+            pltpu.VMEM((width, units), bf16),
+            pltpu.VMEM((width, units), bf16),
+            pltpu.VMEM((units, width), bf16),
+            pltpu.VMEM((depth * count, units), bf16),
+            pltpu.VMEM((QUADS,) + block, bf16),
+            pltpu.VMEM((QUADS,) + block, bf16),
+            pltpu.VMEM((QUADS,) + block, bf16),
+            pltpu.VMEM((2,) + block, bf16),
+            pltpu.VMEM(block, bf16),
+            pltpu.VMEM((depth - 1, count, width), bf16),
+            dma((4,)),
+            dma((ag_sends,)),
+            dma((2 * QUADS, depth)),
+            dma((rs_sends,)),
+            dma((QUADS,)),
+            dma((2, depth)),
+            dma((depth,)),
+            dma((depth - 1,)),
+        ],
+        compiler_params=pltpu.CompilerParams(
+            collective_id=0, has_side_effects=True, vmem_limit_bytes=48 * 2**20
+        ),
+    )(extended, resid_sum, gate_weight, up_weight, down_weight)
+
+
+def routed_experts(
+    resid_sum, normed_rows, routing, route_weights, gate_weight, up_weight, down_weight
+):
+    sp_count = lax.axis_size("sp")
+    row_count = normed_rows.shape[0]
+    capacity = max(2, 2 * TOP * row_count // sp_count)
+    flat_expert = routing.reshape(-1)
+    onehot = (flat_expert[:, None] == jnp.arange(sp_count, dtype=jnp.int32)[None, :]).astype(
+        jnp.int32
+    )
+    earlier = jnp.cumsum(onehot, axis=0) - onehot
+    slot_index = flat_expert * capacity + jnp.sum(earlier * onehot, axis=1)
+    slot_grid = slot_index.reshape(row_count, TOP)
+    slot_ids = jnp.arange(sp_count * capacity, dtype=jnp.int32)
+    placing = jnp.sum(
+        (slot_grid[None, :, :] == slot_ids[:, None, None]).astype(jnp.float32), axis=2
+    ).astype(jnp.bfloat16)
+    outgoing = jnp.dot(placing, normed_rows, preferred_element_type=jnp.float32).astype(
+        jnp.bfloat16
+    )
+    outgoing = outgoing.reshape(sp_count, capacity, normed_rows.shape[1])
+    arrived = lax.all_to_all(outgoing, "sp", split_axis=0, concat_axis=0, tiled=True)
+    row_piece = lax.all_gather(arrived.reshape(-1, arrived.shape[2]), "tp", axis=0, tiled=True)
+    gate_pre = jnp.dot(row_piece, gate_weight[0], preferred_element_type=jnp.float32)
+    up_pre = jnp.dot(row_piece, up_weight[0], preferred_element_type=jnp.float32)
+    hidden = (jax.nn.silu(gate_pre) * up_pre).astype(jnp.bfloat16)
+    summed = lax.psum_scatter(
+        jnp.dot(hidden, down_weight[0], preferred_element_type=jnp.float32).astype(jnp.bfloat16),
+        "tp",
+        scatter_dimension=0,
+        tiled=True,
+    )
+    expert_out = summed.reshape(sp_count, capacity, -1)
+    returned = lax.all_to_all(expert_out, "sp", split_axis=0, concat_axis=0, tiled=True)
+    picked = returned.reshape(sp_count * capacity, -1)[slot_index].astype(jnp.float32)
+    weighted = picked * route_weights.reshape(-1)[:, None]
+    routed = jnp.sum(weighted.reshape(row_count, TOP, -1), axis=1)
+    return (resid_sum + routed).astype(jnp.bfloat16)
 
 
 def on_device(
@@ -128,39 +466,13 @@
         center * lax.rsqrt(jnp.mean(center * center, axis=1, keepdims=True) + 1e-05) * norm_gain
     ).astype(jnp.bfloat16)
     row_count = normed_rows.shape[0]
-    capacity = max(2, 2 * TOP * row_count // sp_count)
-    flat_expert = routing.reshape(-1)
-    onehot = (flat_expert[:, None] == jnp.arange(sp_count, dtype=jnp.int32)[None, :]).astype(
-        jnp.int32
-    )
-    earlier = jnp.cumsum(onehot, axis=0) - onehot
-    slot_index = flat_expert * capacity + jnp.sum(earlier * onehot, axis=1)
-    slot_grid = slot_index.reshape(row_count, TOP)
-    slot_ids = jnp.arange(sp_count * capacity, dtype=jnp.int32)
-    placing = jnp.sum(
-        (slot_grid[None, :, :] == slot_ids[:, None, None]).astype(jnp.float32), axis=2
-    ).astype(jnp.bfloat16)
-    outgoing = jnp.dot(placing, normed_rows, preferred_element_type=jnp.float32).astype(
-        jnp.bfloat16
-    )
-    outgoing = outgoing.reshape(sp_count, capacity, normed_rows.shape[1])
-    arrived = lax.all_to_all(outgoing, "sp", split_axis=0, concat_axis=0, tiled=True)
-    row_piece = lax.all_gather(arrived.reshape(-1, arrived.shape[2]), "tp", axis=0, tiled=True)
-    gate_pre = jnp.dot(row_piece, gate_weight[0], preferred_element_type=jnp.float32)
-    up_pre = jnp.dot(row_piece, up_weight[0], preferred_element_type=jnp.float32)
-    hidden = (jax.nn.silu(gate_pre) * up_pre).astype(jnp.bfloat16)
-    summed = lax.psum_scatter(
-        jnp.dot(hidden, down_weight[0], preferred_element_type=jnp.float32).astype(jnp.bfloat16),
-        "tp",
-        scatter_dimension=0,
-        tiled=True,
-    )
-    expert_out = summed.reshape(sp_count, capacity, -1)
-    returned = lax.all_to_all(expert_out, "sp", split_axis=0, concat_axis=0, tiled=True)
-    picked = returned.reshape(sp_count * capacity, -1)[slot_index].astype(jnp.float32)
-    weighted = picked * route_weights.reshape(-1)[:, None]
-    routed = jnp.sum(weighted.reshape(row_count, TOP, -1), axis=1)
-    return (resid_sum + routed).astype(jnp.bfloat16)
+    if sp_count == QUADS and lax.axis_size("tp") % 4 == 0 and 2 * TOP * row_count // sp_count >= row_count:
+        return dense_experts(
+            resid_sum, normed_rows, routing, route_weights, gate_weight, up_weight, down_weight
+        )
+    return routed_experts(
+        resid_sum, normed_rows, routing, route_weights, gate_weight, up_weight, down_weight
+    )
 
 
 def solution(mesh):

time: 349 us -> 223 us (0.64)
  waiting for transfers between devices: 231 us -> 53.2 us
  Pallas kernels: 0 us -> 117 us
  blocking collectives: 38.8 us -> 9.67 us
  matrix products: 28.8 us -> 6.84 us
  local copies, waits for them, and re-layouts: 18.6 us -> 12.5 us
  other arithmetic: 5.73 us -> 1.83 us
  starting transfers between devices: 8.56 us -> 4.66 us
    pallas_call x0 -> x1, Pallas kernels: none -> 117 us  [dense_experts(): pl.pallas_call(partial(experts_kernel, depth), out_shape=jax.ShapeDtypeSt...]
    reduce_scatter x1 -> x0, waiting for transfers between devices: 88.2 us -> none  [on_device(): lax.psum_scatter(jnp.dot(hidden, down_weight[0], preferred_element_type=j...]
    all_gather x1 -> x0, waiting for transfers between devices: 80 us -> none  [on_device(): lax.all_gather(arrived.reshape(-1, arrived.shape[2]), 'tp', axis=0, tiled...]
    all_to_all x1 -> x0, blocking collectives: 29.2 us -> none  [on_device(): lax.all_to_all(outgoing, 'sp', split_axis=0, concat_axis=0, tiled=True)]
    dot_general x4 -> x0, matrix products: 20.2 us -> none  [the longest x1 7.68 us: on_device(): jnp.dot(row_piece, gate_weight[0], preferred_element_type=jnp.float32)]
    all_to_all x1 -> x0, waiting for transfers between devices: 11.6 us -> none  [on_device(): lax.all_to_all(expert_out, 'sp', split_axis=0, concat_axis=0, tiled=True)]
    all_to_all x1 -> x0, starting transfers between devices: 3.65 us -> none  [on_device(): lax.all_to_all(expert_out, 'sp', split_axis=0, concat_axis=0, tiled=True)]
  transfers between devices with their start and end apart: 6 -> 3, of which waited for: 6 -> 3; matrix products, arithmetic and copies ran while one was open for 2% -> 2% of each run, Pallas kernels for 0% -> 0%
where the time goes in v1:
time: 223 us; the launch traced here: 222 us
  Pallas kernels  117 us (52%)
  waiting for transfers between devices  53.2 us (24%)
  between operations  13.7 us (6%)
  local copies, waits for them, and re-layouts  12.5 us (6%)
  blocking collectives  9.67 us (4%)
  matrix products  6.84 us (3%)
  starting transfers between devices  4.66 us (2%)
  loops' own time  2.56 us (1%)
    pallas_call x1, Pallas kernels, dense_experts(): pl.pallas_call(partial(experts_kernel, depth), out_shape=jax.ShapeDtypeSt...  117 us
    all_gather x1, waiting for transfers between devices, on_device(): lax.all_gather(value_vectors, 'sp', axis=0, tiled=True)  26.6 us
    all_gather x1, waiting for transfers between devices, on_device(): lax.all_gather(key_vectors, 'sp', axis=0, tiled=True)  17.1 us
    all_gather x1, blocking collectives, on_device(): gathered_gates = lax.all_gather(forget_totals, 'sp', axis=0, tiled=True)  9.67 us
    all_to_all x1, waiting for transfers between devices, on_device(): lax.all_to_all(head_out, 'tp', split_axis=0, concat_axis=1, tiled=True)  9.54 us
    unnamed x20, local copies, waits for them, and re-layouts  5.44 us
    dot_general x1, matrix products, on_device(): jnp.dot(token_heads, out_weight, preferred_element_type=jnp.float32)  5.22 us
    all_to_all x1, starting transfers between devices, on_device(): lax.all_to_all(head_out, 'tp', split_axis=0, concat_axis=1, tiled=True)  4.61 us
  transfers between devices with their start and end apart: 3, of which 3 were waited for; matrix products, arithmetic and copies ran while one was open for 2% of the time, Pallas kernels for 0%

profile of v1, /device:TPU:0, one launch (start us, length us, event | category | flops | bytes accessed | tf_op | source)
XLA Modules:
  0.0 222.2 jit_solution(2980634159968988665)
XLA Ops:
  6.5 1.8 copy.41
  8.4 1.8 copy.43
  10.2 1.1 copy.42
  11.5 9.7 %all_gather.9 = f32[2048,2]{0,1:T(2,128)S(1)} all-gather(f32[512,2]{0,1:T(2,128)S(1)} %copy-done.4), channel_id=1, replica_groups=mesh['sp'=4,'tp'=8] {'sp'}, dimensions={0}, use_global_device_ids=true | all-gather | bytes 20480 | tf_op jit(solution)/shard_map/all_gather | solution.py:433
  21.2 17.1 %all-gather.3.cloned.1.call-done = bf16[2048,256]{0,1:T(8,128)(2,1)} async-done(((bf16[512,256]{0,1:T(8,128)(2,1)}), bf16[2048,256]{0,1:T(8,128)(2,1)}) %all-gather.3.cloned.1.call-update) | async-done | bytes 1048592 | tf_op jit(solution)/shard_map/all_gather | solution.py:449
  38.3 1.6 copy.44
  39.9 26.6 %all-gather.5.cloned.1.call-done = bf16[2048,256]{0,1:T(8,128)(2,1)} async-done(((bf16[512,256]{0,1:T(8,128)(2,1)}), bf16[2048,256]{0,1:T(8,128)(2,1)}) %all-gather.5.cloned.1.call-update) | async-done | bytes 1048592 | tf_op jit(solution)/shard_map/all_gather | solution.py:450
  66.5 1.6 copy.46
  68.2 7.2 %while.17 = (s32[]{:T(128)}, f32[2,512]{1,0:T(2,128)S(1)}, f32[2,512]{1,0:T(2,128)S(1)}, f32[2,512,128]{2,1,0:T(8,128)S(1)}, s32[512]{0:T(512)S(1)}, /*index=5*/...) while((s32[]{:T(128)}, f32[2,512]{1,0:T(2,128)S(1)}, ...), condition=%wide.region_5.6_spmd, body=%wide.region_0.5_spmd.sunk | while | flops 274729472 | bytes 9267569 | solution.py:73
  68.2 0.6 slice.8
  69.4 2.3 %conditional.2 = ((f32[2,512]{1,0:T(2,128)S(1)}, f32[2,512]{1,0:T(2,128)S(1)}, f32[2,512,128]{2,1,0:T(8,128)S(1)})) conditional(s32[]{:T(128)} %convert_element_type.44, (f32[2,512]{1,0:T(2,128)S(1)}, f32[2,512]{1,0:T(2,128)S(1)}, f32[2,512,128]{2,1,0:T(8,128)S(1)}) %tuple.49, (s32[]{:T(128)}, s32[512]{0:T(512)S(1)}, s32[512]{0:T(512)S(1)}, ...), branch_computations={%region_1.0_spmd, %region_2.4_spmd} | conditional | flops 274729472 | bytes 9257004 | solution.py:70
  69.6 0.7 fusion.15
  70.4 0.4 fusion.1
  70.8 0.9 convolution_add_fusion
  71.8 0.6 slice.8
  73.0 0.6 slice.8
  74.2 0.6 slice.8
  75.4 0.4 multiply_reduce_fusion.1
  76.5 0.9 convert_element_type.34
  77.3 4.6 %all-to-all-start = ((bf16[8,64,256]{2,1,0:T(8,128)(2,1)}), bf16[8,64,256]{2,1,0:T(8,128)(2,1)S(1)}, u32[]{:S(2)}, u32[]{:S(2)}) async-start(bf16[8,64,256]{2,1,0:T(8,128)(2,1)} %convert_element_type.34), calls=%async_computation | async-start | bytes 524288 | tf_op jit(solution)/shard_map/all_to_all | solution.py:461
  82.1 9.5 %all-to-all-done = bf16[8,64,256]{2,1,0:T(8,128)(2,1)S(1)} async-done(((bf16[8,64,256]{2,1,0:T(8,128)(2,1)}), bf16[8,64,256]{2,1,0:T(8,128)(2,1)S(1)}, u32[]{:S(2)}, u32[]{:S(2)}) %all-to-all-start) | async-done | bytes 262176 | tf_op jit(solution)/shard_map/all_to_all | solution.py:461
  91.7 5.2 %fusion.16 = (f32[64]{0:T(128)S(1)}, f32[64,2048]{1,0:T(8,128)S(1)}) fusion(bf16[64,2048]{1,0:T(8,128)(2,1)S(1)} %bitcast.23, bf16[2048,2048]{1,0:T(8,128)(2,1)} %param.23, bf16[64,2048]{1,0:T(8,128)(2,1)S(1)} %copy-done.2), kind=kOutput, calls=%fused_computation.42 | convolution fusion | flops 537264064 | bytes 9437440 | tf_op jit(solution)/shard_map/dot_general | solution.py:462
  97.4 117.3 %shard_map.127 = bf16[64,2048]{1,0:T(8,128)(2,1)S(1)} custom-call(bf16[64,2176]{1,0:T(8,128)(2,1)S(1)} %fusion.12.own_rows, f32[64,2048]{1,0:T(8,128)S(1)} %get-tuple-element.345.resid, bf16[1,2048,512]{2,1,0:T(8,128)(2,1)S(1)} %copy-done, bf16[1,2048,512]{2,1,0:T(8,128)(2,1)S(1)} %copy-done.1, bf16[1,512,2048]{2,1,0:T(8,128)(2,1)} %down_hbm.1), custom_call_target="tpu_custom_call" | custom-call | tf_op jit(solution)/shard_map/pallas_call | solution.py:342
  214.7 0.7 copy.71
  (55 shorter events, 1.9 us)
Async XLA Ops:
  6.5 5.0 %copy-start.4 = (f32[512,2]{0,1:T(2,128)S(1)}, f32[512,2]{0,1:T(2,128)}, u32[]{:S(2)}) copy-start(f32[512,2]{0,1:T(2,128)} %param.20) | copy-start | bytes 12292
  6.5 31.7 %all-gather.3.cloned.1.call-start = ((), (), s32[]{:S(2)}) async-start(), calls=%async_computation.1 | async-start | bytes 1310720 | tf_op jit(solution)/shard_map/all_gather | solution.py:449
  8.4 58.1 %all-gather.5.cloned.1.call-start = ((), (), s32[]{:S(2)}) async-start(), calls=%async_computation.2 | async-start | bytes 1310720 | tf_op jit(solution)/shard_map/all_gather | solution.py:450
  68.2 7.6 %copy-start.5 = (f32[256]{0:T(256)S(1)}, f32[256]{0:T(256)}, u32[]{:S(2)}) copy-start(f32[256]{0:T(256)} %param.21) | copy-start | bytes 3076
  75.4 6.5 %copy-start.6 = (f32[64,2]{0,1:T(2,128)S(1)}, f32[64,2]{0,1:T(2,128)}, u32[]{:S(2)}) copy-start(f32[64,2]{0,1:T(2,128)} %param.26) | copy-start | bytes 1540
  75.4 6.5 %copy-start.7 = (s32[64,2]{0,1:T(2,128)S(1)}, s32[64,2]{0,1:T(2,128)}, u32[]{:S(2)}) copy-start(s32[64,2]{0,1:T(2,128)} %param.25) | copy-start | bytes 1540
  75.4 16.3 %copy-start.2 = (bf16[64,2048]{1,0:T(8,128)(2,1)S(1)}, bf16[64,2048]{1,0:T(8,128)(2,1)}, u32[]{:S(2)}) copy-start(bf16[64,2048]{1,0:T(8,128)(2,1)} %param.22) | copy-start | bytes 786436
  77.3 14.3 %all-to-all-start = ((bf16[8,64,256]{2,1,0:T(8,128)(2,1)}), bf16[8,64,256]{2,1,0:T(8,128)(2,1)S(1)}, u32[]{:S(2)}, u32[]{:S(2)}) async-start(bf16[8,64,256]{2,1,0:T(8,128)(2,1)} %convert_element_type.34), calls=%async_computation | async-start | bytes 524288 | tf_op jit(solution)/shard_map/all_to_all | solution.py:461
  91.7 5.5 %copy-start.3 = (f32[2048]{0:T(1024)S(1)}, f32[2048]{0:T(1024)}, u32[]{:S(2)}) copy-start(f32[2048]{0:T(1024)} %param.24) | copy-start | bytes 24580
  91.7 5.7 %copy-start = (bf16[1,2048,512]{2,1,0:T(8,128)(2,1)S(1)}, bf16[1,2048,512]{2,1,0:T(8,128)(2,1)}, u32[]{:S(2)}) copy-start(bf16[1,2048,512]{2,1,0:T(8,128)(2,1)} %gate_hbm.1) | copy-start | bytes 6291460
  91.7 5.7 %copy-start.1 = (bf16[1,2048,512]{2,1,0:T(8,128)(2,1)S(1)}, bf16[1,2048,512]{2,1,0:T(8,128)(2,1)}, u32[]{:S(2)}) copy-start(bf16[1,2048,512]{2,1,0:T(8,128)(2,1)} %up_hbm.1) | copy-start | bytes 6291460
Sparse Core Ops, SparseCore 0:
  9.2 29.0 all-gather.2
  40.1 26.3 all-gather.4

commit v2 on v1

--- a/solution.py
+++ b/solution.py
@@ -317,12 +317,208 @@
         copy.wait_send()
 
 
-def dense_experts(
-    resid_sum, normed_rows, routing, route_weights, gate_weight, up_weight, down_weight
+def heads_kernel(
+    queries,
+    keys,
+    values,
+    key_gates,
+    query_gates,
+    gain,
+    stream,
+    out_hbm,
+    norm_gain,
+    pieces,
+    resid_out,
+    rows_out,
+    key_all,
+    value_all,
+    gate_all,
+    peak,
+    weight_total,
+    weighted,
+    leaving,
+    incoming,
+    out_w,
+    local_sem,
+    kv_send_sems,
+    kv_recv_sems,
+    out_send_sems,
+    out_recv_sems,
 ):
-    depth = lax.axis_size("tp") // 2
-    count, width = normed_rows.shape
-    units = gate_weight.shape[2]
+    sp = lax.axis_index("sp")
+    tp = lax.axis_index("tp")
+    tp_count = lax.axis_size("tp")
+    tokens = queries.shape[0]
+    heads = queries.shape[1] // HD
+    width = resid_out.shape[1]
+    count = resid_out.shape[0]
+    core = tp % 2
+    x_next = sp + 1 - 2 * (sp % 2)
+    y_next = (sp + 2) % 4
+    first = x_next * (1 - core) + y_next * core
+    second = y_next * (1 - core) + x_next * core
+    far = 3 - sp
+    load = pltpu.make_async_copy(out_hbm, out_w, local_sem.at[0])
+    load.start()
+
+    barrier = pltpu.get_barrier_semaphore()
+    peers = [(first, tp), (second, tp)]
+    peers += [(sp, (tp + step) % tp_count) for step in range(1, tp_count)]
+    for peer in peers:
+        pl.semaphore_signal(barrier, inc=1, device_id=peer, device_id_type=MESH)
+    pl.semaphore_wait(barrier, len(peers))
+
+    started = []
+
+    def send_block(refs, quad, target):
+        for part, (src, dst) in enumerate(zip(refs, (key_all, value_all, gate_all))):
+            copy = pltpu.make_async_remote_copy(
+                src_ref=src,
+                dst_ref=dst.at[quad],
+                send_sem=kv_send_sems.at[len(started)],
+                recv_sem=kv_recv_sems.at[quad, part],
+                device_id=target,
+                device_id_type=MESH,
+            )
+            copy.start()
+            started.append(copy)
+
+    def block_of(quad):
+        return (key_all.at[quad], value_all.at[quad], gate_all.at[quad])
+
+    def receive_block(quad):
+        for part, ref in enumerate(block_of(quad)):
+            pltpu.make_async_remote_copy(
+                src_ref=ref,
+                dst_ref=ref,
+                send_sem=kv_send_sems.at[0],
+                recv_sem=kv_recv_sems.at[quad, part],
+                device_id=(first, tp),
+                device_id_type=MESH,
+            ).wait_recv()
+
+    chunk = 128
+
+    def attend(refs, diagonal):
+        key_ref, value_ref, gate_ref = refs
+
+        @pl.loop(0, tokens // chunk)
+        def _(j):
+            rows = pl.ds(pl.multiple_of(j * chunk, chunk), chunk)
+            for head in range(heads):
+                cols = slice(head * HD, (head + 1) * HD)
+                scores = lax.dot_general(
+                    queries[rows, cols],
+                    key_ref[:, cols],
+                    (((1,), (1,)), ((), ())),
+                    preferred_element_type=jnp.float32,
+                )
+                scores = (
+                    scores * HD ** (-0.5)
+                    + query_gates[rows, head : head + 1]
+                    - gate_ref[head : head + 1, :]
+                )
+                if diagonal:
+                    row_id = lax.broadcasted_iota(jnp.int32, scores.shape, 0) + j * chunk
+                    col_id = lax.broadcasted_iota(jnp.int32, scores.shape, 1)
+                    scores = jnp.where(col_id <= row_id, scores, masked_score)
+                new_peak = jnp.max(scores, axis=1, keepdims=True)
+                if not diagonal:
+                    old_peak = peak[head, rows]
+                    new_peak = jnp.maximum(old_peak, new_peak)
+                lifted = jnp.exp(scores - new_peak)
+                added = jnp.sum(lifted, axis=1, keepdims=True)
+                product = jnp.dot(
+                    lifted.astype(jnp.bfloat16),
+                    value_ref[:, cols],
+                    preferred_element_type=jnp.float32,
+                )
+                if not diagonal:
+                    rescale = jnp.exp(old_peak - new_peak)
+                    added = weight_total[head, rows] * rescale + added
+                    product = weighted[head, rows] * rescale + product
+                peak[head, rows] = new_peak
+                weight_total[head, rows] = added
+                weighted[head, rows] = product
+
+    def attend_earlier(quad):
+        @pl.when(quad < sp)
+        def _():
+            attend(block_of(quad), False)
+
+    own = (keys, values, key_gates)
+    send_block(own, sp, (first, tp))
+    send_block(own, sp, (second, tp))
+    attend(own, True)
+    receive_block(first)
+    send_block(block_of(first), first, (second, tp))
+    attend_earlier(first)
+    receive_block(second)
+    attend_earlier(second)
+    receive_block(far)
+    attend_earlier(far)
+
+    @pl.loop(0, tp_count)
+    def _(j):
+        rows = pl.ds(pl.multiple_of(j * count, count), count)
+        for head in range(heads):
+            cols = slice(head * HD, (head + 1) * HD)
+            attended = weighted[head, rows] / weight_total[head, rows]
+            square = jnp.mean(attended * attended, axis=1, keepdims=True)
+            normed = attended * lax.rsqrt(square + 1e-06) * gain[0:1, cols]
+            leaving[j, :, cols] = normed.astype(jnp.bfloat16)
+
+    sent = []
+    for step in range(1, tp_count):
+        target = (tp + step) % tp_count
+        copy = pltpu.make_async_remote_copy(
+            src_ref=leaving.at[target],
+            dst_ref=incoming.at[tp],
+            send_sem=out_send_sems.at[step],
+            recv_sem=out_recv_sems.at[tp],
+            device_id=(sp, target),
+            device_id_type=MESH,
+        )
+        copy.start()
+        sent.append(copy)
+    resid_out[...] = stream[...].astype(jnp.float32)
+    load.wait()
+    wide = heads * HD
+    strip = 512 if width % 512 == 0 else width
+    for step in range(tp_count):
+        source = (tp - step + tp_count) % tp_count
+        part = leaving if step == 0 else incoming
+        if step:
+            slot = incoming.at[source]
+            pltpu.make_async_remote_copy(
+                src_ref=slot,
+                dst_ref=slot,
+                send_sem=out_send_sems.at[0],
+                recv_sem=out_recv_sems.at[source],
+                device_id=(first, tp),
+                device_id_type=MESH,
+            ).wait_recv()
+
+        @pl.loop(0, width // strip)
+        def _(j):
+            cols = pl.ds(pl.multiple_of(j * strip, strip), strip)
+            weights = out_w[pl.ds(pl.multiple_of(source * wide, wide), wide), cols]
+            resid_out[:, cols] += jnp.dot(
+                part[source], weights, preferred_element_type=jnp.float32
+            )
+
+    resid = resid_out[...]
+    center = resid - jnp.mean(resid, axis=1, keepdims=True)
+    variance = jnp.mean(center * center, axis=1, keepdims=True)
+    rows_out[:, :width] = (center * lax.rsqrt(variance + 1e-05) * norm_gain[0:1, :]).astype(
+        jnp.bfloat16
+    )
+    rows_out[:, width:] = pieces[...]
+    for copy in started + sent:
+        copy.wait_send()
+
+
+def weight_pieces(routing, route_weights):
     experts = jnp.arange(QUADS, dtype=jnp.int32)
     named = routing[:, :, None] == experts[None, None, :]
     weights = jnp.sum(jnp.where(named, route_weights[:, :, None], 0.0), axis=1)
@@ -330,8 +526,66 @@
     middle = lax.reduce_precision(weights - high, 8, 7)
     low = weights - high - middle
     pieces = jnp.concatenate([high, middle, low], axis=1).astype(jnp.bfloat16)
-    pieces = jnp.pad(pieces, ((0, 0), (0, LANES - pieces.shape[1])))
-    extended = jnp.concatenate([normed_rows, pieces], axis=1)
+    return jnp.pad(pieces, ((0, 0), (0, LANES - pieces.shape[1])))
+
+
+def heads_stage(
+    queries, keys, values, forget_totals, head_gain, stream, out_weight, norm_gain, pieces
+):
+    tokens, wide = queries.shape
+    heads = wide // HD
+    count, width = stream.shape
+    tp_count = lax.axis_size("tp")
+    key_gates = jnp.pad(jnp.transpose(forget_totals), ((0, (-heads) % 8), (0, 0)))
+    bf16, f32 = jnp.bfloat16, jnp.float32
+    dma = pltpu.SemaphoreType.DMA
+    vmem = pl.BlockSpec(memory_space=pltpu.VMEM)
+    hbm = pl.BlockSpec(memory_space=pl.ANY)
+    return pl.pallas_call(
+        heads_kernel,
+        out_shape=(
+            jax.ShapeDtypeStruct((count, width), f32),
+            jax.ShapeDtypeStruct((count, width + LANES), bf16),
+        ),
+        in_specs=[vmem] * 7 + [hbm] + [vmem] * 2,
+        out_specs=(vmem, vmem),
+        scratch_shapes=[
+            pltpu.VMEM((QUADS, tokens, wide), bf16),
+            pltpu.VMEM((QUADS, tokens, wide), bf16),
+            pltpu.VMEM((QUADS,) + key_gates.shape, f32),
+            pltpu.VMEM((heads, tokens, 1), f32),
+            pltpu.VMEM((heads, tokens, 1), f32),
+            pltpu.VMEM((heads, tokens, HD), f32),
+            pltpu.VMEM((tp_count, count, wide), bf16),
+            pltpu.VMEM((tp_count, count, wide), bf16),
+            pltpu.VMEM(out_weight.shape, bf16),
+            dma((1,)),
+            dma((9,)),
+            dma((QUADS, 3)),
+            dma((tp_count,)),
+            dma((tp_count,)),
+        ],
+        compiler_params=pltpu.CompilerParams(
+            collective_id=1, has_side_effects=True, vmem_limit_bytes=40 * 2**20
+        ),
+    )(
+        queries,
+        keys,
+        values,
+        key_gates,
+        forget_totals,
+        head_gain.reshape(1, -1),
+        stream,
+        out_weight,
+        norm_gain.reshape(1, -1),
+        pieces,
+    )
+
+
+def dense_experts(resid_sum, extended, gate_weight, up_weight, down_weight):
+    depth = lax.axis_size("tp") // 2
+    count, width = resid_sum.shape
+    units = gate_weight.shape[2]
     bf16 = jnp.bfloat16
     dma = pltpu.SemaphoreType.DMA
     block = (depth, count, width)
@@ -426,6 +680,21 @@
     up_weight,
     down_weight,
 ):
+    rows_dev, sp_size, tp_size = stream.shape[0], lax.axis_size("sp"), lax.axis_size("tp")
+    dense = 2 * TOP * rows_dev // sp_size >= rows_dev
+    if dense and sp_size == QUADS and tp_size % 4 == 0 and queries.shape[0] % 128 == 0:
+        resid_sum, extended = heads_stage(
+            queries,
+            key_vectors,
+            value_vectors,
+            forget_totals,
+            head_gain,
+            stream,
+            out_weight,
+            norm_gain,
+            weight_pieces(routing, route_weights),
+        )
+        return dense_experts(resid_sum, extended, gate_weight, up_weight, down_weight)
     tok_count = queries.shape[0]
     heads_dev = queries.shape[1] // HD
     sp_index = lax.axis_index("sp")
@@ -465,11 +734,6 @@
     normed_rows = (
         center * lax.rsqrt(jnp.mean(center * center, axis=1, keepdims=True) + 1e-05) * norm_gain
     ).astype(jnp.bfloat16)
-    row_count = normed_rows.shape[0]
-    if sp_count == QUADS and lax.axis_size("tp") % 4 == 0 and 2 * TOP * row_count // sp_count >= row_count:
-        return dense_experts(
-            resid_sum, normed_rows, routing, route_weights, gate_weight, up_weight, down_weight
-        )
     return routed_experts(
         resid_sum, normed_rows, routing, route_weights, gate_weight, up_weight, down_weight
     )

time: 223 us -> 164 us (0.74)
  waiting for transfers between devices: 53.2 us -> 0 us
  Pallas kernels: 117 us -> 152 us
  between operations: 13.7 us -> 0.06 us
  blocking collectives: 9.67 us -> 0 us
  matrix products: 6.84 us -> 0 us
  starting transfers between devices: 4.66 us -> 0 us
  loops' own time: 2.56 us -> 0 us
    all_gather x2 -> x0, waiting for transfers between devices: 43.7 us -> none  [the longest x1 26.6 us: on_device(): lax.all_gather(value_vectors, 'sp', axis=0, tiled=True)]
    pallas_call x0 -> x1, Pallas kernels: none -> 37.6 us  [heads_stage(): pl.pallas_call(heads_kernel, out_shape=(jax.ShapeDtypeStruct((count, widt...]
    all_gather x1 -> x0, blocking collectives: 9.67 us -> none  [on_device(): gathered_gates = lax.all_gather(forget_totals, 'sp', axis=0, tiled=True)]
    all_to_all x1 -> x0, waiting for transfers between devices: 9.54 us -> none  [on_device(): lax.all_to_all(head_out, 'tp', split_axis=0, concat_axis=1, tiled=True)]
    dot_general x3 -> x0, matrix products: 6.84 us -> none  [the longest x1 5.22 us: on_device(): jnp.dot(token_heads, out_weight, preferred_element_type=jnp.float32)]
    unnamed x20, local copies, waits for them, and re-layouts: 5.44 us -> 10.1 us
    all_to_all x1 -> x0, starting transfers between devices: 4.61 us -> none  [on_device(): lax.all_to_all(head_out, 'tp', split_axis=0, concat_axis=1, tiled=True)]
    while x3 -> x0, local copies, waits for them, and re-layouts: 3.4 us -> none  [fold_keys(): return lax.fori_loop(0, key_total // block_len, one_block, state_all)]
  transfers between devices with their start and end apart: 3 -> 0, of which waited for: 3 -> 0; matrix products, arithmetic and copies ran while one was open for 2% -> 0% of each run, Pallas kernels for 0% -> 0%
where the time goes in v2:
time: 164 us; the launch traced here: 163 us
  Pallas kernels  152 us (93%)
  local copies, waits for them, and re-layouts  10.9 us (7%)
    pallas_call x1, Pallas kernels, dense_experts(): pl.pallas_call(partial(experts_kernel, depth), out_shape=jax.ShapeDtypeSt...  114 us
    pallas_call x1, Pallas kernels, heads_stage(): pl.pallas_call(heads_kernel, out_shape=(jax.ShapeDtypeStruct((count, widt...  37.6 us
    unnamed x20, local copies, waits for them, and re-layouts  10.1 us

profile of v2, /device:TPU:0, one launch (start us, length us, event | category | flops | bytes accessed | tf_op | source)
XLA Modules:
  0.0 163.2 jit_solution(8861205480778801418)
XLA Ops:
  0.0 0.7 select_reduce_fusion
  0.7 0.1 copy.21
  0.9 0.7 pad.8.key_gates
  1.5 0.8 copy.22.query_gates
  2.4 0.0 copy-start
  2.4 3.4 %copy-done = bf16[2048,2048]{1,0:T(8,128)(2,1)S(1)} copy-done((bf16[2048,2048]{1,0:T(8,128)(2,1)S(1)}, bf16[2048,2048]{1,0:T(8,128)(2,1)}, u32[]{:S(2)}) %copy-start) | copy-done | bytes 8388632
  5.8 0.0 copy-start.3
  5.8 0.9 copy-done.3
  6.7 0.0 copy-start.4
  6.7 0.9 copy-done.4
  7.7 0.0 copy-start.5
  7.7 0.9 copy-done.5
  8.6 0.0 copy-start.6
  8.6 0.9 copy-done.6
  9.6 0.0 copy-start.7
  9.6 0.7 copy-done.7
  10.3 0.0 copy-start.8
  10.3 0.7 copy-done.8
  10.9 0.0 copy-start.1
  11.0 37.6 %shard_map.127 = (f32[64,2048]{1,0:T(8,128)S(1)}, bf16[64,2176]{1,0:T(8,128)(2,1)S(1)}) custom-call(bf16[512,256]{1,0:T(8,128)(2,1)S(1)} %copy-done.3, bf16[512,256]{1,0:T(8,128)(2,1)S(1)} %copy-done.4, bf16[512,256]{1,0:T(8,128)(2,1)S(1)} %copy-done.5, f32[8,512]{1,0:T(8,128)S(1)} %pad.8.key_gates, f32[512,2]{1,0:T(8,128)S(1)} %copy.22.query_gates, ...), custom_call_target="tpu_custom_call" | custom-call | tf_op jit(solution)/shard_map/pallas_call | solution.py:544
  48.5 0.0 copy-done.1
  48.5 0.0 copy-done.2
  48.5 114.0 %shard_map.128 = bf16[64,2048]{1,0:T(8,128)(2,1)S(1)} custom-call(bf16[64,2176]{1,0:T(8,128)(2,1)S(1)} %get-tuple-element.7.own_rows, f32[64,2048]{1,0:T(8,128)S(1)} %get-tuple-element.8.resid, bf16[1,2048,512]{2,1,0:T(8,128)(2,1)S(1)} %copy-done.1, bf16[1,2048,512]{2,1,0:T(8,128)(2,1)S(1)} %copy-done.2, bf16[1,512,2048]{2,1,0:T(8,128)(2,1)} %down_hbm.1), custom_call_target="tpu_custom_call" | custom-call | tf_op jit(solution)/shard_map/pallas_call | solution.py:596
  162.5 0.7 copy.24
  (4 shorter events, 0.0 us)
Async XLA Ops:
  2.4 3.4 %copy-start = (bf16[2048,2048]{1,0:T(8,128)(2,1)S(1)}, bf16[2048,2048]{1,0:T(8,128)(2,1)}, u32[]{:S(2)}) copy-start(bf16[2048,2048]{1,0:T(8,128)(2,1)} %out_hbm.1) | copy-start | bytes 25165828
  5.8 0.9 copy-start.3
  6.7 0.9 copy-start.4
  7.7 0.9 copy-start.5
  8.6 0.9 copy-start.6
  9.6 0.7 copy-start.7
  10.3 0.7 copy-start.8
  10.9 37.6 %copy-start.1 = (bf16[1,2048,512]{2,1,0:T(8,128)(2,1)S(1)}, bf16[1,2048,512]{2,1,0:T(8,128)(2,1)}, u32[]{:S(2)}) copy-start(bf16[1,2048,512]{2,1,0:T(8,128)(2,1)} %gate_hbm.1) | copy-start | bytes 6291460
  11.0 37.6 %copy-start.2 = (bf16[1,2048,512]{2,1,0:T(8,128)(2,1)S(1)}, bf16[1,2048,512]{2,1,0:T(8,128)(2,1)}, u32[]{:S(2)}) copy-start(bf16[1,2048,512]{2,1,0:T(8,128)(2,1)} %up_hbm.1) | copy-start | bytes 6291460
